TPU v7x, 32 devices: a whole 2x2x4 slice. The times are simulated.
32 devices in a mesh: fs: 8 (over z, x), tp: 4 (over y, core).
Axes of the slice: x: 2, y: 2, z: 4, core: 2. Of those that a mesh axis runs over, the one named last changes fastest.
Arguments:
- stream: bfloat16 [4096, 2048], P('fs', 'tp'), may hold values from -6 to 6
- gain_mix: float32 [2048], replicated, may hold values from 0.1 to 1.9
- pool_weight: bfloat16 [4, 512, 512], P(None, 'fs', 'tp'), may hold values from -0.25 to 0.25
- pool_gain: float32 [2048], replicated, may hold values from 0.1 to 1.9
- gain_ffn: float32 [2048], replicated, may hold values from 0.1 to 1.9
- gate_weight: bfloat16 [2048, 5632], P('fs', 'tp'), may hold values from -0.125 to 0.125
- up_weight: bfloat16 [2048, 5632], P('fs', 'tp'), may hold values from -0.125 to 0.125
- gate_taps: float32 [3, 5632], replicated, may hold values from -2.5 to 2.5
- up_taps: float32 [3, 5632], replicated, may hold values from -2.5 to 2.5
- down_weight: bfloat16 [5632, 2048], P('tp', 'fs'), may hold values from -0.078125 to 0.078125
Outputs:
- layer_out: bfloat16 [4096, 2048], P('fs', 'tp')
All inputs are finite; a program needn't handle non-finite values.
Results may differ from a plain program's by a relative error of at most 0.01.
Values may be sent and summed in bfloat16 or wider, within the bound.
A program may use at most 64 MiB of HBM per device.

v0:
```python
import jax
import jax.numpy as jnp
from jax import lax
from jax.sharding import PartitionSpec as P

LEN = 128
epsilon = 1e-06


def rms_norm(values, scales):
    return values * lax.rsqrt(jnp.mean(values * values, axis=-1, keepdims=True) + epsilon) * scales


def delayed(values, amount):
    return jnp.pad(values, ((0, 0), (amount, 0), (0, 0)))[:, : values.shape[1]]


def pool_less(values):
    channels = values.shape[2]
    group_id = jnp.arange(channels) % 4
    partials = [values]
    running = values
    for amount in (1, 2, 4, 8):
        running = running + delayed(running, amount)
        partials.append(running)
    picked = jnp.where(
        group_id == 0,
        partials[1],
        jnp.where(group_id == 1, partials[2], jnp.where(group_id == 2, partials[3], partials[4])),
    )
    extent = jnp.where(
        group_id == 0, 2.0, jnp.where(group_id == 1, 4.0, jnp.where(group_id == 2, 8.0, 16.0))
    )
    position = jnp.arange(values.shape[1]).astype(jnp.float32)[:, None] + 1.0
    divisor = jnp.minimum(position, extent[None, :])
    return picked / divisor[None] - values


def causal_taps(values, kernel):
    reach = kernel.shape[0]
    length = values.shape[1]
    padded = jnp.pad(values, ((0, 0), (reach - 1, 0), (0, 0)))
    running = padded[:, 0:length] * kernel[0]
    for shift_by in range(1, reach):
        running = running + padded[:, shift_by : shift_by + length] * kernel[shift_by]
    return running


def add_rows(left, portion):
    return jnp.dot(left, portion, preferred_element_type=jnp.float32)


def body(
    stream,
    gain_mix,
    pool_weight,
    pool_gain,
    gain_ffn,
    gate_weight,
    up_weight,
    gate_taps,
    up_taps,
    down_weight,
):
    tok_rows, own_cols = stream.shape
    seq_count = tok_rows // LEN
    gathered = lax.all_gather(stream, "tp", axis=1, tiled=True)
    channels = gathered.shape[1]
    normed = lax.optimization_barrier(
        rms_norm(gathered.astype(jnp.float32), gain_mix).astype(jnp.bfloat16)
    )
    pooled = pool_less(normed.astype(jnp.float32).reshape(seq_count, LEN, channels)).astype(
        jnp.bfloat16
    )
    pooled = pooled.reshape(tok_rows, channels // 4, 4)
    pool_part = lax.all_gather(pool_weight, "fs", axis=1, tiled=True)
    pool_full = lax.all_gather(pool_part, "tp", axis=2, tiled=True)
    mixer = (
        jnp.einsum("tcg,gce->teg", pooled, pool_full, preferred_element_type=jnp.float32).reshape(
            tok_rows, channels
        )
        * pool_gain
    )
    middle = lax.optimization_barrier((gathered.astype(jnp.float32) + mixer).astype(jnp.bfloat16))
    normed_ffn = rms_norm(middle.astype(jnp.float32), gain_ffn).astype(jnp.bfloat16)
    hidden_cols = gate_weight.shape[1]

    def add_single(portion):
        return add_rows(normed_ffn, portion)

    gate_sum = add_single(lax.all_gather(gate_weight, "fs", axis=0, tiled=True))
    value_sum = add_single(lax.all_gather(up_weight, "fs", axis=0, tiled=True))
    gate_proj = lax.optimization_barrier(gate_sum.astype(jnp.bfloat16))
    value_proj = lax.optimization_barrier(value_sum.astype(jnp.bfloat16))
    column_start = lax.axis_index("tp") * hidden_cols
    gate_kernel = lax.dynamic_slice_in_dim(gate_taps, column_start, hidden_cols, 1)
    value_kernel = lax.dynamic_slice_in_dim(up_taps, column_start, hidden_cols, 1)
    gate_conv = causal_taps(
        gate_proj.astype(jnp.float32).reshape(seq_count, LEN, hidden_cols), gate_kernel
    )
    value_conv = causal_taps(
        value_proj.astype(jnp.float32).reshape(seq_count, LEN, hidden_cols), value_kernel
    )
    hidden = (
        (jax.nn.silu(gate_conv) * value_conv).astype(jnp.bfloat16).reshape(tok_rows, hidden_cols)
    )
    partial_value = jnp.dot(
        hidden,
        lax.all_gather(down_weight, "fs", axis=1, tiled=True),
        preferred_element_type=jnp.float32,
    )
    return lax.psum_scatter(partial_value, "tp", scatter_dimension=1, tiled=True).astype(
        jnp.bfloat16
    )


def solution(mesh):
    return jax.shard_map(
        body,
        mesh=mesh,
        in_specs=(
            P("fs", "tp"),
            P(),
            P(None, "fs", "tp"),
            P(),
            P(),
            P("fs", "tp"),
            P("fs", "tp"),
            P(),
            P(),
            P("tp", "fs"),
        ),
        out_specs=P("fs", "tp"),
        check_vma=False,
    )
```

profile of v0, /device:TPU:0, one launch (start us, length us, event | category | flops | bytes accessed | tf_op | source)
XLA Modules:
  0.0 408.1 jit_solution(10271177089141165696)
XLA Ops:
  6.5 0.0 all-gather.6.cloned.1.call-start
  6.5 2.0 copy.16
  8.6 0.0 copy-start.3
  8.6 0.0 all-gather.6.cloned.1.call-update
  8.6 0.0 all-gather.8.cloned.1.call-start
  8.7 0.9 copy.17
  9.6 33.2 %all_gather.19 = bf16[4,512,128]{2,0,1:T(4,128)(2,1)S(1)} all-gather(bf16[4,64,128]{2,0,1:T(4,128)(2,1)S(1)} %copy.17), channel_id=1, replica_groups=mesh['fs'=8,'tp'=4] {'fs'}, dimensions={1}, use_global_device_ids=true | all-gather | bytes 589824 | tf_op jit(solution)/shard_map/all_gather | solution.py:76
  42.7 1.1 copy.18
  43.9 0.0 all-gather.8.cloned.1.call-update
  43.9 0.0 all-gather.10.cloned.1.call-start
  43.9 0.7 all-gather.10.cloned.1.call-update
  44.6 0.0 all-gather.12.cloned.1.call-start
  44.7 0.5 all-gather.12.cloned.1.call-update
  45.2 0.0 all-gather.14.cloned.1.call-start
  45.2 0.5 all-gather.14.cloned.1.call-update
  45.8 0.0 reduce-scatter.2.cloned.1.call-start
  45.8 1.0 dynamic-slice_reduce_fusion.2
  46.9 0.3 broadcast_minimum_fusion
  47.2 0.0 all-gather.6.cloned.1.call-done
  47.2 2.1 fusion.3
  49.4 0.0 copy-done.3
  49.4 2.2 fusion.5
  51.5 3.1 reshape.110
  54.6 5.6 %fusion.9 = f32[4,128,2048]{1,0,2:T(4,128)S(1)} fusion(f32[4,128,2048]{1,0,2:T(4,128)} %reshape.110), kind=kLoop, calls=%fused_computation.20 | loop fusion | flops 1048576 | bytes 8388608 | tf_op jit(solution)/shard_map/add | solution.py:24
  60.3 2.3 fusion.10
  62.6 0.0 copy-start
  62.6 2.3 fusion.11
  65.0 0.0 copy-done
  65.0 16.9 %fusion.12 = bf16[4,128,2048]{1,0,2:T(4,128)(2,1)} fusion(f32[4,128,2048]{1,0,2:T(4,128)S(1)} %copy-done, f32[4,128,2048]{1,0,2:T(4,128)S(1)} %fusion.9, f32[4,128,2048]{1,0,2:T(4,128)S(1)} %fusion.11, f32[128,2048]{0,1:T(8,128)S(1)} %broadcast_minimum_fusion, pred[2048]{0:T(1024)(128)(4,1)S(1)} %get-tuple-element.11, ...), kind=kLoop, calls=%fused_computation.23 | loop fusion | flops 8388608 | bytes 15734784 | tf_op jit(solution)/shard_map/convert_element_type | solution.py:72
  81.9 2.7 reshape.102
  84.7 0.0 all-gather.8.cloned.1.call-done
  84.7 3.0 convolution_bitcast_fusion
  87.7 4.8 %copy.20 = f32[512,512,4]{0,2,1:T(4,128)} copy(f32[512,512,4]{0,1,2:T(8,128)S(1)} %convolution_bitcast_fusion) | data formatting | bytes 8388608 | tf_op jit(solution)/shard_map/tcg,gce->teg/transpose | solution.py:79
  92.4 0.0 copy-start.1
  92.4 0.0 copy-start.4
  92.4 5.5 %reshape.103 = f32[512,2048]{0,1:T(8,128)} reshape(f32[512,512,4]{0,2,1:T(4,128)} %copy.20) | data formatting | bytes 8388608 | tf_op jit(solution)/shard_map/reshape | solution.py:79
  97.9 0.0 copy-done.1
  97.9 0.0 copy-done.4
  97.9 0.0 copy-start.5
  97.9 2.7 fusion.6
  100.7 0.0 copy-start.2
  100.7 1.3 copy-done.2
  102.0 0.5 fusion
  102.5 59.6 %all-gather.10.cloned.1.call-done = bf16[2048,1408]{1,0:T(8,128)(2,1)} async-done(((bf16[256,1408]{1,0:T(8,128)(2,1)}), bf16[2048,1408]{1,0:T(8,128)(2,1)}) %all-gather.10.cloned.1.call-update) | async-done | bytes 5767184 | tf_op jit(solution)/shard_map/all_gather | solution.py:91
  162.1 0.0 copy-done.5
  162.1 6.9 %convolution_convert_fusion.1 = bf16[512,1408]{1,0:T(8,128)(2,1)S(1)} fusion(bf16[2048,1408]{1,0:T(8,128)(2,1)} %all-gather.10.cloned.1.call-done, bf16[512,2048]{0,1:T(8,128)(2,1)} %copy-done.2, f32[2048]{0:T(1024)S(1)} %copy-done.5, f32[512]{0:T(512)S(1)} %add_rsqrt_fusion), kind=kOutput, calls=%fused_computation.25 | convolution fusion | flops 2957705216 | bytes 9316352 | tf_op jit(solution)/shard_map/dot_general | solution.py:50
  169.0 0.2 convert.3
  169.2 85.4 %all-gather.12.cloned.1.call-done = bf16[2048,1408]{1,0:T(8,128)(2,1)} async-done(((bf16[256,1408]{1,0:T(8,128)(2,1)}), bf16[2048,1408]{1,0:T(8,128)(2,1)}) %all-gather.12.cloned.1.call-update) | async-done | bytes 5767184 | tf_op jit(solution)/shard_map/all_gather | solution.py:92
  254.6 6.9 %convolution_convert_fusion = bf16[512,1408]{1,0:T(8,128)(2,1)S(1)} fusion(bf16[2048,1408]{1,0:T(8,128)(2,1)} %all-gather.12.cloned.1.call-done, bf16[512,2048]{0,1:T(8,128)(2,1)} %copy-done.2, f32[2048]{0:T(1024)S(1)} %copy-done.5, f32[512]{0:T(512)S(1)} %add_rsqrt_fusion), kind=kOutput, calls=%fused_computation.24 | convolution fusion | flops 2957705216 | bytes 9316352 | tf_op jit(solution)/shard_map/dot_general | solution.py:50
  261.6 0.2 convert.4
  261.8 3.3 fusion.21
  265.1 82.8 %all-gather.14.cloned.1.call-done = bf16[1408,2048]{1,0:T(8,128)(2,1)} async-done(((bf16[1408,256]{1,0:T(8,128)(2,1)}), bf16[1408,2048]{1,0:T(8,128)(2,1)}) %all-gather.14.cloned.1.call-update) | async-done | bytes 5767184 | tf_op jit(solution)/shard_map/all_gather | solution.py:109
  347.9 8.5 %fusion.32 = f32[512,2048]{1,0:T(8,128)} fusion(bf16[512,1408]{1,0:T(8,128)(2,1)} %bitcast.18, bf16[1408,2048]{1,0:T(8,128)(2,1)} %all-gather.14.cloned.1.call-done), kind=kOutput, calls=%fused_computation.61 | convolution fusion | flops 2952790016 | bytes 11403264 | tf_op jit(solution)/shard_map/dot_general | solution.py:107
  356.4 0.0 reduce-scatter.2.cloned.1.call-update
  356.4 42.7 %reduce-scatter.2.cloned.1.call-done = f32[512,512]{1,0:T(8,128)} async-done(((f32[512,2048]{1,0:T(8,128)}), f32[512,512]{1,0:T(8,128)}) %reduce-scatter.2.cloned.1.call-update) | async-done | bytes 1048592 | tf_op jit(solution)/shard_map/reduce_scatter | solution.py:112
  399.2 2.1 convert_element_type.62
  (6 shorter events, 0.0 us)
Async XLA Ops:
  6.5 40.7 %all-gather.6.cloned.1.call-start = ((), (), s32[]{:S(2)}) async-start(), calls=%async_computation.1 | async-start | bytes 2621440 | tf_op jit(solution)/shard_map/all_gather | solution.py:67
  8.6 40.8 %copy-start.3 = (f32[2048]{0:T(1024)S(1)}, f32[2048]{0:T(1024)}, u32[]{:S(2)}) copy-start(f32[2048]{0:T(1024)} %param.11) | copy-start | bytes 24580
  8.6 76.1 %all-gather.8.cloned.1.call-start = ((), (), s32[]{:S(2)}) async-start(), calls=%async_computation.2 | async-start | bytes 2621440 | tf_op jit(solution)/shard_map/all_gather | solution.py:77
  43.9 118.2 %all-gather.10.cloned.1.call-start = ((), (), s32[]{:S(2)}) async-start(), calls=%async_computation.3 | async-start | bytes 6488064 | tf_op jit(solution)/shard_map/all_gather | solution.py:91
  44.6 210.0 %all-gather.12.cloned.1.call-start = ((), (), s32[]{:S(2)}) async-start(), calls=%async_computation.4 | async-start | bytes 6488064 | tf_op jit(solution)/shard_map/all_gather | solution.py:92
  45.2 302.7 %all-gather.14.cloned.1.call-start = ((), (), s32[]{:S(2)}) async-start(), calls=%async_computation.5 | async-start | bytes 6488064 | tf_op jit(solution)/shard_map/all_gather | solution.py:109
  45.8 353.4 %reduce-scatter.2.cloned.1.call-start = ((), (), s32[]{:S(2)}) async-start(), calls=%async_computation.6 | async-start | bytes 5242880 | tf_op jit(solution)/shard_map/reduce_scatter | solution.py:112
  62.6 2.3 copy-start
  92.4 5.5 %copy-start.1 = (bf16[512,2048]{0,1:T(8,128)(2,1)S(1)}, bf16[512,2048]{0,1:T(8,128)(2,1)}, u32[]{:S(2)}) copy-start(bf16[512,2048]{0,1:T(8,128)(2,1)} %all-gather.6.cloned.1.call-done) | copy-start | bytes 6291460
  92.4 5.5 %copy-start.4 = (f32[2048]{0:T(1024)S(1)}, f32[2048]{0:T(1024)}, u32[]{:S(2)}) copy-start(f32[2048]{0:T(1024)} %param.13) | copy-start | bytes 24580
  97.9 64.2 %copy-start.5 = (f32[2048]{0:T(1024)S(1)}, f32[2048]{0:T(1024)}, u32[]{:S(2)}) copy-start(f32[2048]{0:T(1024)} %param.14) | copy-start | bytes 24580
  100.7 1.3 copy-start.2
Sparse Core Ops, SparseCore 0:
  8.9 25.2 all-gather.5
  44.0 23.5 all-gather.7
  69.7 92.2 all-gather.9
  164.1 90.4 all-gather.11
  256.5 91.2 all-gather.13
  356.5 42.5 reduce-scatter.1
where the time goes:
time: 409 us; the launch traced here: 408 us
  waiting for transfers between devices  272 us (67%)
  other arithmetic  41 us (10%)
  blocking collectives  33.2 us (8%)
  matrix products  25.3 us (6%)
  local copies, waits for them, and re-layouts  22.5 us (6%)
  between operations  13.6 us (3%)
    all_gather x1, waiting for transfers between devices, body(): value_sum = add_single(lax.all_gather(up_weight, 'fs', axis=0, tiled=True))  85.4 us
    all_gather x1, waiting for transfers between devices, body(): lax.all_gather(down_weight, 'fs', axis=1, tiled=True)  82.8 us
    all_gather x1, waiting for transfers between devices, body(): gate_sum = add_single(lax.all_gather(gate_weight, 'fs', axis=0, tiled=True))  59.6 us
    reduce_scatter x1, waiting for transfers between devices, body(): lax.psum_scatter(partial_value, 'tp', scatter_dimension=1, tiled=True)  42.7 us
    all_gather x1, blocking collectives, body(): pool_part = lax.all_gather(pool_weight, 'fs', axis=1, tiled=True)  33.2 us
    convert_element_type x1, other arithmetic, body(): pool_less(normed.astype(jnp.float32).reshape(seq_count, LEN, channels))  16.9 us
    dot_general x2, matrix products, add_rows(): return jnp.dot(left, portion, preferred_element_type=jnp.float32)  13.8 us
    add x3, other arithmetic, pool_less(): running = running + delayed(running, amount)  10.3 us
  transfers between devices with their start and end apart: 6, of which 4 were waited for; matrix products, arithmetic and copies ran while one was open for 18% of the time, Pallas kernels for 0%

commit v1 on v0

--- a/solution.py
+++ b/solution.py
@@ -62,6 +62,36 @@
     up_taps,
     down_weight,
 ):
+
+    def switch_table_in(own_rows, u_in):
+        mesh_dim = "tp"
+        row_out, frame_out, res = (
+            lax.axis_size(mesh_dim),
+            lax.axis_index(mesh_dim),
+            own_rows.shape[2],
+        )
+        upper, s_next = ([], [])
+        a_next = current_block = own_rows
+        for j0 in range(row_out // 2 + 1):
+            upper.append(u_in(a_next, (frame_out - j0) % row_out * res))
+            if 0 < j0 < row_out - row_out // 2:
+                s_next.append(u_in(current_block, (frame_out + j0) % row_out * res))
+            a_next = lax.ppermute(
+                a_next,
+                axis_name=mesh_dim,
+                perm=list(map(lambda no: (no, (no + 1) % row_out), range(row_out))),
+            )
+            current_block = lax.ppermute(
+                current_block,
+                axis_name=mesh_dim,
+                perm=list(map(lambda no: (no, (no - 1) % row_out), range(row_out))),
+            )
+        return jnp.roll(
+            jnp.concatenate([*upper[::-1], *s_next], axis=1),
+            (frame_out - row_out // 2) * upper[0].shape[1],
+            1,
+        )
+
     tok_rows, own_cols = stream.shape
     seq_count = tok_rows // LEN
     gathered = lax.all_gather(stream, "tp", axis=1, tiled=True)
@@ -74,11 +104,13 @@
     )
     pooled = pooled.reshape(tok_rows, channels // 4, 4)
     pool_part = lax.all_gather(pool_weight, "fs", axis=1, tiled=True)
-    pool_full = lax.all_gather(pool_part, "tp", axis=2, tiled=True)
     mixer = (
-        jnp.einsum("tcg,gce->teg", pooled, pool_full, preferred_element_type=jnp.float32).reshape(
-            tok_rows, channels
-        )
+        switch_table_in(
+            pool_part,
+            lambda shard, offset: jnp.einsum(
+                "tcg,gce->teg", pooled, shard, preferred_element_type=jnp.float32
+            ),
+        ).reshape(tok_rows, channels)
         * pool_gain
     )
     middle = lax.optimization_barrier((gathered.astype(jnp.float32) + mixer).astype(jnp.bfloat16))

time: 409 us -> 375 us (0.917)
  waiting for transfers between devices: 272 us -> 231 us
  matrix products: 25.3 us -> 29.7 us
    all_gather x1, waiting for transfers between devices: 59.6 us -> 8.54 us  [body(): gate_sum = add_single(lax.all_gather(gate_weight, 'fs', axis=0, tiled=True))]
    ppermute x0 -> x3, waiting for transfers between devices: none -> 9.5 us  [the longest x2 9.49 us: switch_table_in(): lax.ppermute(a_next, axis_name=mesh_dim, perm=list(map(lambda no: (no, (n...]
    dynamic_slice x0 -> x2, local copies, waits for them, and re-layouts: none -> 5.16 us  [switch_table_in(): jnp.roll(jnp.concatenate([*upper[::-1], *s_next], axis=1), (frame_out - r...]
    transpose x1 -> x0, local copies, waits for them, and re-layouts: 4.76 us -> none  [body(): jnp.einsum('tcg,gce->teg', pooled, pool_full, preferred_element_type=jnp....]
    dot_general x1 -> x4, matrix products: 2.97 us -> 7.41 us  [body(): jnp.einsum('tcg,gce->teg', pooled, shard, preferred_element_type=jnp.floa...]
  transfers between devices with their start and end apart: 6 -> 8, of which waited for: 4 -> 5; matrix products, arithmetic and copies ran while one was open for 18% -> 22% of each run, Pallas kernels for 0% -> 0%
where the time goes in v1:
time: 375 us
  waiting for transfers between devices  231 us (62%)
  other arithmetic  40.1 us (11%)
  blocking collectives  33.1 us (9%)
  matrix products  29.7 us (8%)
  local copies, waits for them, and re-layouts  25.6 us (7%)
  between operations  13.4 us (4%)
    all_gather x1, waiting for transfers between devices, body(): value_sum = add_single(lax.all_gather(up_weight, 'fs', axis=0, tiled=True))  85.6 us
    all_gather x1, waiting for transfers between devices, body(): lax.all_gather(down_weight, 'fs', axis=1, tiled=True)  82.7 us
    reduce_scatter x1, waiting for transfers between devices, body(): lax.psum_scatter(partial_value, 'tp', scatter_dimension=1, tiled=True)  42.7 us
    all_gather x1, blocking collectives, body(): pool_part = lax.all_gather(pool_weight, 'fs', axis=1, tiled=True)  33.1 us
    convert_element_type x1, other arithmetic, body(): pool_less(normed.astype(jnp.float32).reshape(seq_count, LEN, channels))  16.2 us
    dot_general x2, matrix products, add_rows(): return jnp.dot(left, portion, preferred_element_type=jnp.float32)  13.8 us
    add x3, other arithmetic, pool_less(): running = running + delayed(running, amount)  10.2 us
    ppermute x2, waiting for transfers between devices, switch_table_in(): lax.ppermute(a_next, axis_name=mesh_dim, perm=list(map(lambda no: (no, (n...  9.49 us
  transfers between devices with their start and end apart: 8, of which 5 were waited for; matrix products, arithmetic and copies ran while one was open for 22% of the time, Pallas kernels for 0%

profile of v1, /device:TPU:0, one launch (start us, length us, event | category | flops | bytes accessed | tf_op | source)
XLA Modules:
  0.0 374.5 jit_solution(12065762510770101453)
XLA Ops:
  6.5 0.0 copy-start.3
  6.5 0.0 all-gather.5.cloned.1.call-start
  6.5 2.1 copy.21
  8.6 0.0 all-gather.5.cloned.1.call-update
  8.6 0.0 all-gather.7.cloned.1.call-start
  8.7 0.7 all-gather.7.cloned.1.call-update
  9.4 0.0 all-gather.9.cloned.1.call-start
  9.4 0.7 all-gather.9.cloned.1.call-update
  10.1 0.0 all-gather.11.cloned.1.call-start
  10.2 0.9 copy.22
  11.1 33.1 %all_gather.16 = bf16[4,512,128]{2,0,1:T(4,128)(2,1)S(1)} all-gather(bf16[4,64,128]{2,0,1:T(4,128)(2,1)S(1)} %copy.22), channel_id=1, replica_groups=mesh['fs'=8,'tp'=4] {'fs'}, dimensions={1}, use_global_device_ids=true | all-gather | bytes 589824 | tf_op jit(solution)/shard_map/all_gather | solution.py:106
  44.2 1.1 copy.23
  45.3 0.0 collective-permute-start
  45.3 1.7 collective-permute-start.2
  47.1 0.0 all-gather.11.cloned.1.call-update
  47.1 0.0 reduce-scatter.2.cloned.1.call-start
  47.2 1.0 dynamic-slice_reduce_fusion.2
  48.2 0.3 broadcast_minimum_fusion
  48.6 9.5 %collective-permute-done = bf16[4,512,128]{1,2,0:T(8,128)(2,1)} collective-permute-done((bf16[4,512,128]{1,2,0:T(8,128)(2,1)}, bf16[4,512,128]{1,2,0:T(8,128)(2,1)}, u32[]{:S(2)}, u32[]{:S(2)}) %collective-permute-start) | collective-permute-done | bytes 524320 | tf_op jit(solution)/shard_map/ppermute | solution.py:79
  58.1 0.2 collective-permute-start.1
  58.2 2.1 fusion.3
  60.3 0.0 copy-done.3
  60.3 2.1 fusion.5
  62.5 3.0 reshape.110
  65.5 5.5 %fusion.9 = f32[4,128,2048]{1,0,2:T(4,128)S(1)} fusion(f32[4,128,2048]{1,0,2:T(4,128)} %reshape.110), kind=kLoop, calls=%fused_computation.20 | loop fusion | flops 1048576 | bytes 8388608 | tf_op jit(solution)/shard_map/add | solution.py:24
  71.0 2.3 fusion.10
  73.3 0.0 copy-start
  73.4 2.3 fusion.11
  75.7 0.0 copy-done
  75.7 16.2 %fusion.12 = bf16[4,128,2048]{1,0,2:T(4,128)(2,1)S(1)} fusion(f32[4,128,2048]{1,0,2:T(4,128)S(1)} %copy-done, f32[4,128,2048]{1,0,2:T(4,128)S(1)} %fusion.9, f32[4,128,2048]{1,0,2:T(4,128)S(1)} %fusion.11, f32[128,2048]{0,1:T(8,128)S(1)} %broadcast_minimum_fusion, pred[2048]{0:T(1024)(128)(4,1)S(1)} %get-tuple-element.19, ...), kind=kLoop, calls=%fused_computation.23 | loop fusion | flops 8388608 | bytes 15734784 | tf_op jit(solution)/shard_map/convert_element_type | solution.py:102
  91.9 2.2 reshape.102
  94.1 3.0 copy.24
  97.1 0.0 collective-permute-done.1
  97.1 1.9 constant_dynamic-update-slice_fusion.7
  99.0 1.8 constant_dynamic-update-slice_fusion.6
  100.8 1.9 constant_dynamic-update-slice_fusion.5
  102.7 0.0 collective-permute-done.2
  102.7 1.9 constant_dynamic-update-slice_fusion.4
  104.5 0.1 constant_dynamic-update-slice_fusion.3
  104.6 0.1 constant_dynamic-update-slice_fusion.2
  104.7 0.1 constant_dynamic-update-slice_fusion.1
  104.8 0.1 constant_dynamic-update-slice_fusion
  104.9 0.4 constant_dynamic-slice_fusion
  105.3 4.7 %copy.30 = f32[512,512,4]{0,2,1:T(4,128)} copy(f32[512,512,4]{0,1,2:T(8,128)S(1)} %constant_dynamic-slice_fusion) | data formatting | bytes 8388608 | tf_op jit(solution)/shard_map/jit(_roll_dynamic)/dynamic_slice | solution.py:89
  110.1 5.5 %reshape.103 = f32[512,2048]{0,1:T(8,128)} reshape(f32[512,512,4]{0,2,1:T(4,128)} %copy.30) | data formatting | bytes 8388608 | tf_op jit(solution)/shard_map/reshape | solution.py:113
  115.6 0.0 copy-done.1
  115.6 0.0 copy-done.4
  115.6 2.7 fusion.6
  118.3 0.0 copy-start.2
  118.3 1.3 copy-done.2
  119.7 0.5 fusion
  120.2 8.5 %all-gather.7.cloned.1.call-done = bf16[2048,1408]{1,0:T(8,128)(2,1)} async-done(((bf16[256,1408]{1,0:T(8,128)(2,1)}), bf16[2048,1408]{1,0:T(8,128)(2,1)}) %all-gather.7.cloned.1.call-update) | async-done | bytes 5767184 | tf_op jit(solution)/shard_map/all_gather | solution.py:123
  128.7 0.0 copy-done.5
  128.7 6.9 %convolution_convert_fusion.1 = bf16[512,1408]{1,0:T(8,128)(2,1)S(1)} fusion(bf16[2048,1408]{1,0:T(8,128)(2,1)} %all-gather.7.cloned.1.call-done, bf16[512,2048]{0,1:T(8,128)(2,1)} %copy-done.2, f32[2048]{0:T(1024)S(1)} %copy-done.5, f32[512]{0:T(512)S(1)} %add_rsqrt_fusion), kind=kOutput, calls=%fused_computation.25 | convolution fusion | flops 2957705216 | bytes 9316352 | tf_op jit(solution)/shard_map/dot_general | solution.py:50
  135.6 0.2 convert.3
  135.9 85.6 %all-gather.9.cloned.1.call-done = bf16[2048,1408]{1,0:T(8,128)(2,1)} async-done(((bf16[256,1408]{1,0:T(8,128)(2,1)}), bf16[2048,1408]{1,0:T(8,128)(2,1)}) %all-gather.9.cloned.1.call-update) | async-done | bytes 5767184 | tf_op jit(solution)/shard_map/all_gather | solution.py:124
  221.4 6.9 %convolution_convert_fusion = bf16[512,1408]{1,0:T(8,128)(2,1)S(1)} fusion(bf16[2048,1408]{1,0:T(8,128)(2,1)} %all-gather.9.cloned.1.call-done, bf16[512,2048]{0,1:T(8,128)(2,1)} %copy-done.2, f32[2048]{0:T(1024)S(1)} %copy-done.5, f32[512]{0:T(512)S(1)} %add_rsqrt_fusion), kind=kOutput, calls=%fused_computation.24 | convolution fusion | flops 2957705216 | bytes 9316352 | tf_op jit(solution)/shard_map/dot_general | solution.py:50
  228.4 0.2 convert.4
  228.6 3.4 fusion.21
  232.0 82.7 %all-gather.11.cloned.1.call-done = bf16[1408,2048]{1,0:T(8,128)(2,1)} async-done(((bf16[1408,256]{1,0:T(8,128)(2,1)}), bf16[1408,2048]{1,0:T(8,128)(2,1)}) %all-gather.11.cloned.1.call-update) | async-done | bytes 5767184 | tf_op jit(solution)/shard_map/all_gather | solution.py:141
  314.7 8.4 %fusion.31 = f32[512,2048]{1,0:T(8,128)} fusion(bf16[512,1408]{1,0:T(8,128)(2,1)} %bitcast.31, bf16[1408,2048]{1,0:T(8,128)(2,1)} %all-gather.11.cloned.1.call-done), kind=kOutput, calls=%fused_computation.72 | convolution fusion | flops 2952790016 | bytes 11403264 | tf_op jit(solution)/shard_map/dot_general | solution.py:139
  323.1 0.0 reduce-scatter.2.cloned.1.call-update
  323.2 42.7 %reduce-scatter.2.cloned.1.call-done = f32[512,512]{1,0:T(8,128)} async-done(((f32[512,2048]{1,0:T(8,128)}), f32[512,512]{1,0:T(8,128)}) %reduce-scatter.2.cloned.1.call-update) | async-done | bytes 1048592 | tf_op jit(solution)/shard_map/reduce_scatter | solution.py:144
  365.9 2.1 convert_element_type.62
  (10 shorter events, 0.1 us)
Async XLA Ops:
  6.5 53.8 %copy-start.3 = (f32[2048]{0:T(1024)S(1)}, f32[2048]{0:T(1024)}, u32[]{:S(2)}) copy-start(f32[2048]{0:T(1024)} %param.11) | copy-start | bytes 24580
  6.5 51.7 %all-gather.5.cloned.1.call-start = ((), (), s32[]{:S(2)}) async-start(), calls=%async_computation.1 | async-start | bytes 2621440 | tf_op jit(solution)/shard_map/all_gather | solution.py:97
  8.6 120.1 %all-gather.7.cloned.1.call-start = ((), (), s32[]{:S(2)}) async-start(), calls=%async_computation.2 | async-start | bytes 6488064 | tf_op jit(solution)/shard_map/all_gather | solution.py:123
  9.4 212.1 %all-gather.9.cloned.1.call-start = ((), (), s32[]{:S(2)}) async-start(), calls=%async_computation.3 | async-start | bytes 6488064 | tf_op jit(solution)/shard_map/all_gather | solution.py:124
  10.1 304.6 %all-gather.11.cloned.1.call-start = ((), (), s32[]{:S(2)}) async-start(), calls=%async_computation.4 | async-start | bytes 6488064 | tf_op jit(solution)/shard_map/all_gather | solution.py:141
  45.3 12.7 %collective-permute-start = (bf16[4,512,128]{1,2,0:T(8,128)(2,1)}, bf16[4,512,128]{1,2,0:T(8,128)(2,1)}, u32[]{:S(2)}, u32[]{:S(2)}) collective-permute-start(bf16[4,512,128]{1,2,0:T(8,128)(2,1)} %copy.23), channel_id=1, source_target_pairs={{0,1},{1,2},{2,3},{3,0},{4,5},{5,6},{6,7},{7,4},{8,9},{9,10},{10,1... | collective-permute-start | bytes 1572872 | tf_op jit(solution)/shard_map/ppermute | solution.py:79
  45.3 57.3 %collective-permute-start.2 = (bf16[4,512,128]{1,2,0:T(8,128)(2,1)}, bf16[4,512,128]{1,2,0:T(8,128)(2,1)}, u32[]{:S(2)}, u32[]{:S(2)}) collective-permute-start(bf16[4,512,128]{1,2,0:T(8,128)(2,1)} %copy.23), channel_id=1, source_target_pairs={{0,3},{1,0},{2,1},{3,2},{4,7},{5,4},{6,5},{7,6},{8,11},{9,8},{10,9... | collective-permute-start | bytes 1572872 | tf_op jit(solution)/shard_map/ppermute | solution.py:84
  47.1 318.8 %reduce-scatter.2.cloned.1.call-start = ((), (), s32[]{:S(2)}) async-start(), calls=%async_computation.5 | async-start | bytes 5242880 | tf_op jit(solution)/shard_map/reduce_scatter | solution.py:144
  58.1 39.0 %collective-permute-start.1 = (bf16[4,512,128]{1,2,0:T(8,128)(2,1)}, bf16[4,512,128]{1,2,0:T(8,128)(2,1)}, u32[]{:S(2)}, u32[]{:S(2)}) collective-permute-start(bf16[4,512,128]{1,2,0:T(8,128)(2,1)} %collective-permute-done), channel_id=1, source_target_pairs={{0,1},{1,2},{2,3},{3,0},{4,5},{5,6},{6,7},{7,4},{8,9},{9,10},{10,1... | collective-permute-start | bytes 1572872 | tf_op jit(solution)/shard_map/ppermute | solution.py:79
  73.3 2.3 copy-start
  110.0 5.5 %copy-start.1 = (bf16[512,2048]{0,1:T(8,128)(2,1)S(1)}, bf16[512,2048]{0,1:T(8,128)(2,1)}, u32[]{:S(2)}) copy-start(bf16[512,2048]{0,1:T(8,128)(2,1)} %all-gather.5.cloned.1.call-done) | copy-start | bytes 6291460
  110.0 5.5 %copy-start.4 = (f32[2048]{0:T(1024)S(1)}, f32[2048]{0:T(1024)}, u32[]{:S(2)}) copy-start(f32[2048]{0:T(1024)} %param.13) | copy-start | bytes 24580
  115.6 13.2 %copy-start.5 = (f32[2048]{0:T(1024)S(1)}, f32[2048]{0:T(1024)}, u32[]{:S(2)}) copy-start(f32[2048]{0:T(1024)} %param.14) | copy-start | bytes 24580
  118.3 1.3 copy-start.2
Sparse Core Ops, SparseCore 0:
  8.9 25.2 all-gather.4
  36.4 92.2 all-gather.6
  130.9 90.4 all-gather.8
  223.3 91.3 all-gather.10
  323.3 42.5 reduce-scatter.1
